TPU v7x, 512 devices: a whole 4x8x8 slice. The times are simulated.
512 devices in a mesh: kv: 64 (over z, y), tp: 8 (over x, core).
Axes of the slice: x: 4, y: 8, z: 8, core: 2. Of those that a mesh axis runs over, the one named last changes fastest.
Arguments:
- tokens: bfloat16 [128, 4096], P(None, 'kv'), may hold values from -16 to 16
- mix_gain: bfloat16 [4096], P('kv'), may hold values from 0.099609375 to 1.8984375
- ffn_gain: bfloat16 [4096], P('kv'), may hold values from 0.099609375 to 1.8984375
- w_query: bfloat16 [4096, 2048], P('kv', 'tp'), may hold values from -0.09375 to 0.09375
- w_key: bfloat16 [4096, 2048], P('kv', 'tp'), may hold values from -0.09375 to 0.09375
- w_value: bfloat16 [4096, 4096], P('kv', 'tp'), may hold values from -0.09375 to 0.09375
- w_gate: bfloat16 [4096, 4096], P('kv', 'tp'), may hold values from -0.09375 to 0.09375
- w_decay: bfloat16 [4096, 2048], P('kv', 'tp'), may hold values from -0.375 to 0.375
- decay_bias: float32 [2048], P('tp'), may hold values from -7 to 4
- head_gain: bfloat16 [512], replicated, may hold values from 0.099609375 to 1.8984375
- w_output: bfloat16 [4096, 4096], P('tp', 'kv'), may hold values from -0.09375 to 0.09375
- w_ffgate: bfloat16 [4096, 11008], P('kv', 'tp'), may hold values from -0.09375 to 0.09375
- w_ffup: bfloat16 [4096, 11008], P('kv', 'tp'), may hold values from -0.09375 to 0.09375
- w_down: bfloat16 [11008, 4096], P('tp', 'kv'), may hold values from -0.0546875 to 0.0546875
- state: float32 [128, 8, 256, 512], P('kv', 'tp'), may hold values from -6 to 6
Outputs:
- mixed: bfloat16 [128, 4096], P(None, 'kv')
- new_state: float32 [128, 8, 256, 512], P('kv', 'tp')
All inputs are finite; a program needn't handle non-finite values.
Results may differ from a plain program's by a relative error of at most 0.015.
Values may be sent and summed in bfloat16 or wider, within the bound.
No kernel may reach another device: no remote copies, remote signals or barrier semaphores. Data moves between devices by JAX's collectives and lax.ppermute only.
A program may use at most 64 MiB of HBM per device.

v0:
```python
import functools

import jax
import jax.numpy as jnp
from jax import lax
from jax.experimental import pallas as pl
from jax.experimental.pallas import tpu as pltpu
from jax.sharding import PartitionSpec as P

epsilon = 1e-06


STRIDE = 8


def member(kv):
    place = kv // STRIDE
    return (place ^ (place >> 2)) & 1


def lines(kv):
    return [[i for i in range(kv) if member(i) == m] for m in range(2)]


def pairs(kv, tp):
    return [
        [i * tp + t for i in sorted((j, j ^ STRIDE), key=member) for t in range(tp)]
        for j in range(kv)
        if j < j ^ STRIDE
    ]


def padded(n):
    return -(-n // 128) * 128


def in_vmem(x):
    return pltpu.with_memory_space_constraint(x, pltpu.VMEM)


def whole(count):
    return [pl.BlockSpec(memory_space=pltpu.VMEM)] * count


def widths(units):
    half = units // 2
    return half, padded(2 * half + 1), padded(half)


def fetch(sources, held, sems):
    copies = [pltpu.make_async_copy(a, b, sems.at[i]) for i, (a, b) in enumerate(zip(sources, held))]
    for c in copies:
        c.start()
    return copies


def project_kernel(*refs, count, kept):
    sources, out_ref = (refs[:count], refs[count])
    held = refs[count + 1 + kept : -1] + refs[count + 1 : count + 1 + kept]
    copies = fetch(sources, held, refs[-1])
    for copy in copies:
        copy.wait()
    tok, gain = held[:2]
    x = tok[...].astype(jnp.float32).T
    mix_in = (x * gain[...].astype(jnp.float32)).astype(jnp.bfloat16)
    at = 0
    for w in held[2 : count - kept]:
        n = w.shape[1]
        part = jnp.dot(mix_in, w[...], preferred_element_type=jnp.float32)
        out_ref[:, at : at + n] = part.astype(jnp.bfloat16)
        at += n
    squares = jnp.sum(x * x, axis=1, keepdims=True)
    rest = out_ref.shape[1] - at
    lane = lax.broadcasted_iota(jnp.int32, (x.shape[0], rest), 1)
    out_ref[:, at:] = jnp.where(lane == 0, squares, 0.0).astype(jnp.bfloat16)


def project(tok_t, gain, weights, kept):
    total = sum(w.shape[1] for w in weights)
    arrays = (tok_t, gain, *weights, *kept)
    return pl.pallas_call(
        functools.partial(project_kernel, count=len(arrays), kept=len(kept)),
        out_shape=(
            pltpu.VMEM((tok_t.shape[1], total + 128), jnp.bfloat16),
            *(pltpu.VMEM(a.shape, a.dtype) for a in kept),
        ),
        in_specs=[pl.BlockSpec(memory_space=pl.ANY)] * len(arrays),
        out_specs=whole(1 + len(kept)),
        scratch_shapes=[pltpu.VMEM(a.shape, a.dtype) for a in arrays[: len(arrays) - len(kept)]]
        + [pltpu.SemaphoreType.DMA((len(arrays),))],
        name="project",
    )(*arrays)


def pack_kernel(_, tok, ffn_gain, *refs):
    splits, (mine_ref, sent_ref) = (refs[:-2], refs[-2:])
    rows, units = splits[0].shape
    seqs = tok.shape[1]
    half, both, alone = widths(units)

    def fill(ref, m, first):
        gate, up, down = (w[:, m * half : (m + 1) * half] for w in splits)
        ref[:, :half] = gate
        ref[:, half : 2 * half] = up
        ref[:, 2 * half : both] = jnp.zeros((rows, both - 2 * half), ref.dtype)
        ref[:, both : both + half] = down
        ref[:, both + half : both + alone] = jnp.zeros((rows, alone - half), ref.dtype)
        end = both + alone
        ref[:, end : end + seqs] = tok[...]
        ref[:, end + seqs :] = jnp.zeros((rows, 2 * rows), ref.dtype)
        side = 0 if first else rows
        ref[0:1, end + seqs + side : end + seqs + side + rows] = ffn_gain[...]

    for m in range(2):

        @pl.when(member(lax.axis_index("kv")) == m)
        def _():
            fill(mine_ref, m, True)
            fill(sent_ref, 1 - m, False)


def pack(after, tok_t, ffn_gain, splits):
    width, rows = tok_t.shape
    lanes = sum(widths(splits[0].shape[1])[1:]) + rows + 2 * width
    arrays = (after, tok_t, ffn_gain, *splits)
    return pl.pallas_call(
        pack_kernel,
        out_shape=(pltpu.VMEM((width, lanes), jnp.bfloat16),) * 2,
        in_specs=whole(len(arrays)),
        out_specs=whole(2),
        compiler_params=pltpu.CompilerParams(vmem_limit_bytes=8 << 20),
        name="pack",
    )(*(in_vmem(a) for a in arrays))


def attend_kernel(sums, bias, gain, state, key_ref, value_ref, decay_ref, out_ref, *, model_width):
    rows, _, kd, vd = state.shape
    base = sums[...]
    rms = lax.rsqrt(base[:, 3 * kd + 2 * vd : 3 * kd + 2 * vd + 1] / model_width + epsilon)
    q = base[:, :kd] * rms * kd**-0.5
    k = base[:, kd : 2 * kd] * rms
    v = base[:, 2 * kd : 2 * kd + vd] * rms
    g = base[:, 2 * kd + vd : 2 * kd + 2 * vd] * rms
    x = base[:, 2 * kd + 2 * vd : 3 * kd + 2 * vd] * rms + bias[...]
    log_sigmoid = jnp.minimum(x, 0.0) - jnp.log1p(jnp.exp(-jnp.abs(x)))
    decay = jnp.exp(log_sigmoid / 16.0)
    key_ref[...] = k
    value_ref[...] = v
    decay_ref[...] = decay
    fresh = jnp.sum(q * k, axis=1, keepdims=True) * v
    columns = jnp.concatenate([q * decay, jnp.zeros((8 - rows, kd), jnp.float32)], axis=0).T
    step = 32
    found = []
    for s in range(rows):
        total = jnp.zeros((8, vd), jnp.float32)
        for at in range(0, kd, step):
            read = columns[at : at + step, s : s + 1] * state[s, 0, at : at + step]
            total = total + jnp.sum(read.reshape(step // 8, 8, vd), axis=0)
        found.append(jnp.sum(total, axis=0, keepdims=True))
    attended = jnp.concatenate(found, axis=0) + fresh
    scale = lax.rsqrt(jnp.sum(attended * attended, axis=1, keepdims=True) / vd + epsilon)
    gains = jnp.concatenate([gain[i : i + 1] for i in range(gain.shape[0])], axis=1)
    gated = attended * scale * gains.astype(jnp.float32) * (g / (1.0 + jnp.exp(-g)))
    out_ref[...] = jnp.broadcast_to(gated.astype(jnp.bfloat16)[None], out_ref.shape)


def attend(sums, bias, gain, state, model_width, copies):
    rows, _, kd, vd = state.shape
    return pl.pallas_call(
        functools.partial(attend_kernel, model_width=model_width),
        out_shape=(
            pltpu.VMEM((rows, kd), jnp.float32),
            pltpu.VMEM((rows, vd), jnp.float32),
            pltpu.VMEM((rows, kd), jnp.float32),
            jax.ShapeDtypeStruct((copies, rows, vd), jnp.bfloat16),
        ),
        in_specs=whole(4),
        out_specs=whole(4),
        compiler_params=pltpu.CompilerParams(vmem_limit_bytes=8 << 20),
        name="attend",
    )(*(in_vmem(a) for a in (sums, bias, gain, state)))


def join_kernel(heads, weights, out_ref):
    made = lax.dot_general(
        weights[...], heads[...], (((1,), (1,)), ((), ())), preferred_element_type=jnp.float32
    ).astype(jnp.bfloat16)
    for j in range(out_ref.shape[0]):
        out_ref[j] = made


def join(heads, weights, copies):
    return pl.pallas_call(
        join_kernel,
        out_shape=pltpu.VMEM((copies, weights.shape[0], heads.shape[0]), jnp.bfloat16),
        in_specs=whole(2),
        out_specs=pl.BlockSpec(memory_space=pltpu.VMEM),
        compiler_params=pltpu.CompilerParams(vmem_limit_bytes=8 << 20),
        name="join",
    )(*(in_vmem(a) for a in (heads, weights)))


def total_kernel(parts, out_ref):
    out_ref[...] = jnp.sum(parts[...].astype(jnp.float32), axis=1)


def total(parts):
    return pl.pallas_call(
        total_kernel,
        out_shape=pltpu.VMEM((parts.shape[0], *parts.shape[2:]), jnp.float32),
        in_specs=whole(1),
        out_specs=pl.BlockSpec(memory_space=pltpu.VMEM),
        compiler_params=pltpu.CompilerParams(vmem_limit_bytes=8 << 20),
        name="total",
    )(in_vmem(parts))


def widen_kernel(parts, mine, got, _, out_ref, mid_ref, *, alone):
    r = member(lax.axis_index("kv"))
    _, seqs = mid_ref.shape
    both = out_ref.shape[-1]
    end = both + alone

    def mid_of(ref, at):
        return (ref[:, end : end + seqs].astype(jnp.float32) + parts[at]).astype(jnp.bfloat16)

    own = mid_of(mine, r)
    mid_ref[...] = own
    x = jnp.concatenate([own, mid_of(got, 1 - r)], axis=0).astype(jnp.float32).T
    gains = mine[0:1, end + seqs :].astype(jnp.float32) + got[0:1, end + seqs :].astype(jnp.float32)
    ffn_in = (x * gains).astype(jnp.bfloat16)
    squares = jnp.sum(x * x, axis=1, keepdims=True)
    weights = jnp.concatenate([mine[:, :both], got[:, :both]], axis=0)
    made = jnp.dot(ffn_in, weights, preferred_element_type=jnp.float32)
    lane = lax.broadcasted_iota(jnp.int32, (seqs, 128), 1)
    last = jnp.where(lane == 127, squares, made[:, both - 128 :])
    made = jnp.concatenate([made[:, : both - 128], last], axis=1)
    copies, per, _ = out_ref.shape
    for i in range(2):
        rows = made[i * seqs // 2 : (i + 1) * seqs // 2].reshape(copies, per // 2, both)
        out_ref[:, i * per // 2 : (i + 1) * per // 2] = rows.astype(jnp.bfloat16)


def widen(parts, mine, got, new_state, units, count):
    width, seqs = parts.shape[1:]
    _, both, alone = widths(units)
    return pl.pallas_call(
        functools.partial(widen_kernel, alone=alone),
        out_shape=(
            pltpu.VMEM((count, seqs // count, both), jnp.bfloat16),
            pltpu.VMEM((width, seqs), jnp.bfloat16),
        ),
        in_specs=whole(4),
        out_specs=whole(2),
        compiler_params=pltpu.CompilerParams(vmem_limit_bytes=8 << 20),
        name="widen",
    )(*(in_vmem(a) for a in (parts, mine, got, new_state)))


def gate_kernel(sums, out_ref, *, half, model_width):
    rows, both = sums.shape
    rms = lax.rsqrt(sums[:, both - 1 :] / model_width + epsilon)
    gate = sums[:, :half] * rms
    up = sums[:, half : 2 * half] * rms
    hidden = gate / (1.0 + jnp.exp(-gate)) * up
    beside = jnp.concatenate([hidden[: rows // 2], hidden[rows // 2 :]], axis=1)
    out_ref[...] = jnp.broadcast_to(beside.astype(jnp.bfloat16)[None], out_ref.shape)


def gate_units(sums, units, model_width, copies):
    half = units // 2
    return pl.pallas_call(
        functools.partial(gate_kernel, half=half, model_width=model_width),
        out_shape=pltpu.VMEM((copies, sums.shape[0] // 2, 2 * half), jnp.bfloat16),
        in_specs=whole(1),
        out_specs=pl.BlockSpec(memory_space=pltpu.VMEM),
        compiler_params=pltpu.CompilerParams(vmem_limit_bytes=8 << 20),
        name="gate",
    )(in_vmem(sums))


def narrow_kernel(hidden, mine, got, out_ref, *, both):
    r = member(lax.axis_index("kv"))
    half = hidden.shape[1] // 2
    copies, width = out_ref.shape[1:3]
    weights = jnp.concatenate([ref[:, both : both + half] for ref in (mine, got)], axis=0)
    ordered = jnp.concatenate([hidden[:, :half], hidden[:, half:]], axis=0)
    made = lax.dot_general(
        weights, ordered, (((1,), (1,)), ((), ())), preferred_element_type=jnp.float32
    ).astype(jnp.bfloat16)
    for j in range(copies):
        out_ref[r, j] = made[:width]
        out_ref[1 - r, j] = made[width:]


def narrow(hidden, mine, got, units, tp):
    width, seqs = (mine.shape[0], 2 * hidden.shape[0])
    return pl.pallas_call(
        functools.partial(narrow_kernel, both=widths(units)[1]),
        out_shape=pltpu.VMEM((2, tp, width, seqs), jnp.bfloat16),
        in_specs=whole(3),
        out_specs=pl.BlockSpec(memory_space=pltpu.VMEM),
        compiler_params=pltpu.CompilerParams(vmem_limit_bytes=8 << 20),
        name="narrow",
    )(*(in_vmem(a) for a in (hidden, mine, got)))


def exchanged(blocks, axis, groups=None):
    return lax.all_to_all(blocks, axis, 0, 0, axis_index_groups=groups, tiled=True)


def summed(blocks):
    return jnp.sum(blocks.astype(jnp.float32), axis=0)


def local(
    tokens,
    mix_gain,
    ffn_gain,
    w_query,
    w_key,
    w_value,
    w_gate,
    w_decay,
    decay_bias,
    head_gain,
    w_output,
    w_ffgate,
    w_ffup,
    w_down,
    state,
):
    own_rows, heads, _, val_dim = state.shape
    kv, tp = (lax.axis_size(a) for a in ("kv", "tp"))
    model_width = tokens.shape[1] * kv
    made, bias, head_scale, ffn_scale = project(
        tokens.T,
        mix_gain[None, :],
        (w_query, w_key, w_value, w_gate, w_decay),
        (decay_bias[None, :], head_gain.reshape(-1, 128), ffn_gain[None, :]),
    )
    arrived = exchanged(made.reshape(kv, own_rows, -1), "kv")
    keys, values, decay, head_out = attend(
        summed(arrived), bias, head_scale, state, model_width, kv
    )
    heads_all = exchanged(head_out, "kv")
    mine, sent = pack(keys, tokens.T, ffn_scale, (w_ffgate, w_ffup, w_down.T))
    got = lax.ppermute(sent, "kv", [(i, i ^ STRIDE) for i in range(kv)])
    new_state = (
        decay[:, None, :, None] * state + keys[:, None, :, None] * values[:, None, None, :]
    )
    heads_all = heads_all.reshape(-1, heads * val_dim)
    attn_copies = join(heads_all, w_output.T, 2 * tp)
    attn_copies, new_state = lax.optimization_barrier((attn_copies, new_state))
    width, seqs = attn_copies.shape[1:]
    pair, line = (pairs(kv, tp), lines(kv))
    attn_parts = exchanged(attn_copies, ("kv", "tp"), pair)
    units = w_ffgate.shape[1]
    attn_sums = total(attn_parts.reshape(2, tp, width, seqs))
    count = len(line[0])
    wide, mid_t = widen(attn_sums, mine, got, new_state, units, count)
    sums = summed(exchanged(wide, "kv", line))
    hidden = exchanged(gate_units(sums, units, model_width, count), "kv", line)
    down_parts = narrow(hidden.reshape(-1, units), mine, got, units, tp).reshape(2 * tp, width, seqs)
    mixed = (
        mid_t.astype(jnp.float32) + summed(exchanged(down_parts, ("kv", "tp"), pair))
    ).astype(jnp.bfloat16)
    return (mixed.T, new_state)


def solution(mesh):
    in_specs = (
        P(None, "kv"),
        P("kv"),
        P("kv"),
        P("kv", "tp"),
        P("kv", "tp"),
        P("kv", "tp"),
        P("kv", "tp"),
        P("kv", "tp"),
        P("tp"),
        P(),
        P("tp", "kv"),
        P("kv", "tp"),
        P("kv", "tp"),
        P("tp", "kv"),
        P("kv", "tp", None, None),
    )
    out_specs = (P(None, "kv"), P("kv", "tp", None, None))
    return jax.shard_map(local, mesh=mesh, in_specs=in_specs, out_specs=out_specs, check_vma=False)
```

profile of v0, /device:TPU:1, one launch (start us, length us, event | category | flops | bytes accessed | tf_op | source)
XLA Modules:
  0.0 126.0 jit_solution(5145221209678558436)
XLA Ops:
  0.6 1.4 %project.1 = (bf16[128,1920]{1,0:T(8,128)(2,1)S(1)}, f32[1,256]{1,0:T(1,128)S(1)}, bf16[4,128]{1,0:T(4,128)(2,1)S(1)}, bf16[1,64]{1,0:T(2,128)(2,1)S(1)}) custom-call(bf16[64,128]{1,0:T(8,128)(2,1)} %bitcast.15, bf16[1,64]{1,0:T(2,128)(2,1)} %bitcast.19, bf16[64,256]{1,0:T(8,128)(2,1)} %refs_2_.1, bf16[64,256]{1,0:T(8,128)(2,1)} %refs_3_.1, ...), custom_call_target="tpu_custom_call" | custom-call | tf_op jit(solution)/shard_map/project/pallas_call | solution.py:81
  2.0 0.0 copy-start
  2.0 0.2 reshape.36
  2.2 33.8 %all_to_all.30 = bf16[64,2,1920]{2,1,0:T(2,128)(2,1)S(1)} all-to-all(bf16[64,2,1920]{2,1,0:T(2,128)(2,1)S(1)} %reshape.36), channel_id=1, replica_groups=mesh['kv'=64,'tp'=8] {'kv'}, dimensions={0} | all-to-all | bytes 983040 | tf_op jit(solution)/shard_map/all_to_all | solution.py:309
  36.0 0.4 convert_reduce_fusion.sums
  36.5 0.0 copy-done
  36.5 1.2 attend.1
  37.6 6.5 %all-to-all-start.1 = ((bf16[64,2,512]{2,1,0:T(2,128)(2,1)}), bf16[64,2,512]{2,1,0:T(2,128)(2,1)S(1)}, u32[]{:S(2)}, u32[]{:S(2)}) async-start(bf16[64,2,512]{2,1,0:T(2,128)(2,1)} %get-tuple-element.19), calls=%async_computation.1 | async-start | bytes 262144 | tf_op jit(solution)/shard_map/all_to_all | solution.py:309
  44.1 0.2 multiply_add_fusion._
  44.4 0.0 copy-start.1
  44.4 0.0 copy-start.5
  44.4 11.3 %all-to-all-done.1 = bf16[64,2,512]{2,1,0:T(2,128)(2,1)S(1)} async-done(((bf16[64,2,512]{2,1,0:T(2,128)(2,1)}), bf16[64,2,512]{2,1,0:T(2,128)(2,1)S(1)}, u32[]{:S(2)}, u32[]{:S(2)}) %all-to-all-start.1) | async-done | bytes 131104 | tf_op jit(solution)/shard_map/all_to_all | solution.py:309
  55.7 0.1 reshape.37.heads
  55.8 0.0 copy-done.5
  55.8 0.0 copy-start.4
  55.8 0.9 join.1
  56.6 0.0 copy-start.2
  56.7 0.0 copy-start.3
  56.7 0.0 copy-start.6
  56.7 7.4 %all-to-all-start.2 = ((bf16[16,64,128]{2,1,0:T(8,128)(2,1)}), bf16[16,64,128]{2,1,0:T(8,128)(2,1)S(1)}, u32[]{:S(2)}, u32[]{:S(2)}) async-start(bf16[16,64,128]{2,1,0:T(8,128)(2,1)} %join.1), calls=%async_computation.2 | async-start | bytes 524288 | tf_op jit(solution)/shard_map/all_to_all | solution.py:309
  64.1 0.0 copy-done.4
  64.1 0.0 copy-done.2
  64.1 0.0 copy-done.3
  64.1 0.0 copy-done.6
  64.1 0.2 pack.1
  64.3 3.3 %collective-permute-start = (bf16[64,2432]{1,0:T(8,128)(2,1)S(1)}, bf16[64,2432]{1,0:T(8,128)(2,1)S(1)}, u32[]{:S(2)}, u32[]{:S(2)}) collective-permute-start(bf16[64,2432]{1,0:T(8,128)(2,1)S(1)} %get-tuple-element.26), channel_id=1, source_target_pairs={{0,64},{8,72},{16,80},{24,88},{32,96},{40,104},{48,112},{56,120},{... | collective-permute-start | bytes 933896 | tf_op jit(solution)/shard_map/ppermute | solution.py:348
  67.5 3.8 %all-to-all-done.2 = bf16[16,64,128]{2,1,0:T(8,128)(2,1)S(1)} async-done(((bf16[16,64,128]{2,1,0:T(8,128)(2,1)}), bf16[16,64,128]{2,1,0:T(8,128)(2,1)S(1)}, u32[]{:S(2)}, u32[]{:S(2)}) %all-to-all-start.2) | async-done | bytes 262176 | tf_op jit(solution)/shard_map/all_to_all | solution.py:309
  71.3 4.4 %collective-permute-done.got = bf16[64,2432]{1,0:T(8,128)(2,1)S(1)} collective-permute-done((bf16[64,2432]{1,0:T(8,128)(2,1)S(1)}, bf16[64,2432]{1,0:T(8,128)(2,1)S(1)}, u32[]{:S(2)}, u32[]{:S(2)}) %collective-permute-start) | collective-permute-done | bytes 311328 | tf_op jit(solution)/shard_map/ppermute | solution.py:348
  75.8 0.0 copy-done.1
  75.8 0.6 widen.1
  76.3 15.7 %all_to_all.31 = bf16[32,4,1408]{2,1,0:T(4,128)(2,1)S(1)} all-to-all(bf16[32,4,1408]{2,1,0:T(4,128)(2,1)S(1)} %get-tuple-element.29), channel_id=1, replica_groups={{0,8,16,24,32,40,48,56,128,136,144,152,160,168,176,184,320,328,336,344,..., dimensions={0} | all-to-all | bytes 720896 | tf_op jit(solution)/shard_map/all_to_all | solution.py:309
  92.1 0.2 convert_reduce_fusion.1.sums
  92.2 0.2 gate.1
  92.5 18.1 %all_to_all.32 = bf16[32,2,1376]{2,1,0:T(2,128)(2,1)S(1)} all-to-all(bf16[32,2,1376]{2,1,0:T(2,128)(2,1)S(1)} %gate.1), channel_id=1, replica_groups={{0,8,16,24,32,40,48,56,128,136,144,152,160,168,176,184,320,328,336,344,..., dimensions={0} | all-to-all | bytes 352256 | tf_op jit(solution)/shard_map/all_to_all | solution.py:309
  110.6 0.1 reshape.39.hidden
  110.8 0.3 narrow.1
  111.1 14.3 %all_to_all.33 = bf16[16,64,128]{2,1,0:T(8,128)(2,1)S(1)} all-to-all(bf16[16,64,128]{2,1,0:T(8,128)(2,1)S(1)} %bitcast.12), channel_id=1, replica_groups={{0,1,2,3,4,5,6,7,64,65,66,67,68,69,70,71},{8,9,10,11,12,13,14,15,72,73,..., dimensions={0} | all-to-all | bytes 524288 | tf_op jit(solution)/shard_map/all_to_all | solution.py:309
  125.4 0.6 fusion
  (2 shorter events, 0.1 us)
Async XLA Ops:
  2.0 34.4 %copy-start = (f32[2,1,256,512]{3,2,1,0:T(8,128)S(1)}, f32[2,1,256,512]{3,2,1,0:T(8,128)}, u32[]{:S(2)}) copy-start(f32[2,1,256,512]{3,2,1,0:T(8,128)} %state.1) | copy-start | bytes 3145732
  37.6 18.0 %all-to-all-start.1 = ((bf16[64,2,512]{2,1,0:T(2,128)(2,1)}), bf16[64,2,512]{2,1,0:T(2,128)(2,1)S(1)}, u32[]{:S(2)}, u32[]{:S(2)}) async-start(bf16[64,2,512]{2,1,0:T(2,128)(2,1)} %get-tuple-element.19), calls=%async_computation.1 | async-start | bytes 262144 | tf_op jit(solution)/shard_map/all_to_all | solution.py:309
  44.4 31.4 %copy-start.1 = (f32[2,1,256,512]{3,2,1,0:T(8,128)}, f32[2,1,256,512]{3,2,1,0:T(8,128)S(1)}, u32[]{:S(2)}) copy-start(f32[2,1,256,512]{3,2,1,0:T(8,128)S(1)} %multiply_add_fusion._) | copy-start | bytes 3145732
  44.4 11.4 %copy-start.5 = (bf16[512,64]{0,1:T(8,128)(2,1)S(1)}, bf16[512,64]{0,1:T(8,128)(2,1)}, u32[]{:S(2)}) copy-start(bf16[512,64]{0,1:T(8,128)(2,1)} %param.25) | copy-start | bytes 196612
  55.8 8.3 %copy-start.4 = (bf16[1376,64]{0,1:T(8,128)(2,1)S(1)}, bf16[1376,64]{0,1:T(8,128)(2,1)}, u32[]{:S(2)}) copy-start(bf16[1376,64]{0,1:T(8,128)(2,1)} %param.28) | copy-start | bytes 528388
  56.6 7.4 %copy-start.2 = (bf16[64,1376]{1,0:T(8,128)(2,1)S(1)}, bf16[64,1376]{1,0:T(8,128)(2,1)}, u32[]{:S(2)}) copy-start(bf16[64,1376]{1,0:T(8,128)(2,1)} %refs_0_.1) | copy-start | bytes 528388
  56.7 7.4 %copy-start.3 = (bf16[64,1376]{1,0:T(8,128)(2,1)S(1)}, bf16[64,1376]{1,0:T(8,128)(2,1)}, u32[]{:S(2)}) copy-start(bf16[64,1376]{1,0:T(8,128)(2,1)} %refs_1_.1) | copy-start | bytes 528388
  56.7 7.4 %copy-start.6 = (bf16[128,64]{0,1:T(8,128)(2,1)S(1)}, bf16[128,64]{0,1:T(8,128)(2,1)}, u32[]{:S(2)}) copy-start(bf16[128,64]{0,1:T(8,128)(2,1)} %param.15) | copy-start | bytes 49156
  56.7 14.6 %all-to-all-start.2 = ((bf16[16,64,128]{2,1,0:T(8,128)(2,1)}), bf16[16,64,128]{2,1,0:T(8,128)(2,1)S(1)}, u32[]{:S(2)}, u32[]{:S(2)}) async-start(bf16[16,64,128]{2,1,0:T(8,128)(2,1)} %join.1), calls=%async_computation.2 | async-start | bytes 524288 | tf_op jit(solution)/shard_map/all_to_all | solution.py:309
  64.3 11.5 %collective-permute-start = (bf16[64,2432]{1,0:T(8,128)(2,1)S(1)}, bf16[64,2432]{1,0:T(8,128)(2,1)S(1)}, u32[]{:S(2)}, u32[]{:S(2)}) collective-permute-start(bf16[64,2432]{1,0:T(8,128)(2,1)S(1)} %get-tuple-element.26), channel_id=1, source_target_pairs={{0,64},{8,72},{16,80},{24,88},{32,96},{40,104},{48,112},{56,120},{... | collective-permute-start | bytes 933896 | tf_op jit(solution)/shard_map/ppermute | solution.py:348
where the time goes:
time: 127 us; the launch traced here: 126 us
  blocking collectives  81.9 us (64%)
  waiting for transfers between devices  19.5 us (15%)
  starting transfers between devices  17.2 us (14%)
  Pallas kernels  4.72 us (4%)
  other arithmetic  1.44 us (1%)
    all_to_all x4, blocking collectives, exchanged(): lax.all_to_all(blocks, axis, 0, 0, axis_index_groups=groups, tiled=True)  81.9 us
    all_to_all x2, waiting for transfers between devices, exchanged(): lax.all_to_all(blocks, axis, 0, 0, axis_index_groups=groups, tiled=True)  15.1 us
    all_to_all x2, starting transfers between devices, exchanged(): lax.all_to_all(blocks, axis, 0, 0, axis_index_groups=groups, tiled=True)  13.9 us
    ppermute x1, waiting for transfers between devices, local(): got = lax.ppermute(sent, 'kv', [(i, i ^ STRIDE) for i in range(kv)])  4.43 us
    ppermute x1, starting transfers between devices, local(): got = lax.ppermute(sent, 'kv', [(i, i ^ STRIDE) for i in range(kv)])  3.26 us
  transfers between devices with their start and end apart: 3, of which 3 were waited for; matrix products, arithmetic and copies ran while one was open for 0% of the time, Pallas kernels for 0%

commit v1 on v0

--- a/solution.py
+++ b/solution.py
@@ -58,11 +58,13 @@
     sources, out_ref = (refs[:count], refs[count])
     held = refs[count + 1 + kept : -1] + refs[count + 1 : count + 1 + kept]
     copies = fetch(sources, held, refs[-1])
-    for copy in copies:
+    for copy in copies[:2]:
         copy.wait()
     tok, gain = held[:2]
     x = tok[...].astype(jnp.float32).T
     mix_in = (x * gain[...].astype(jnp.float32)).astype(jnp.bfloat16)
+    for copy in copies[2:]:
+        copy.wait()
     at = 0
     for w in held[2 : count - kept]:
         n = w.shape[1]
@@ -235,10 +237,7 @@
     lane = lax.broadcasted_iota(jnp.int32, (seqs, 128), 1)
     last = jnp.where(lane == 127, squares, made[:, both - 128 :])
     made = jnp.concatenate([made[:, : both - 128], last], axis=1)
-    copies, per, _ = out_ref.shape
-    for i in range(2):
-        rows = made[i * seqs // 2 : (i + 1) * seqs // 2].reshape(copies, per // 2, both)
-        out_ref[:, i * per // 2 : (i + 1) * per // 2] = rows.astype(jnp.bfloat16)
+    out_ref[...] = made.reshape(out_ref.shape).astype(jnp.bfloat16)
 
 
 def widen(parts, mine, got, new_state, units, count):
@@ -259,19 +258,20 @@
 
 def gate_kernel(sums, out_ref, *, half, model_width):
     rows, both = sums.shape
+    alone = out_ref.shape[-1]
     rms = lax.rsqrt(sums[:, both - 1 :] / model_width + epsilon)
     gate = sums[:, :half] * rms
     up = sums[:, half : 2 * half] * rms
     hidden = gate / (1.0 + jnp.exp(-gate)) * up
-    beside = jnp.concatenate([hidden[: rows // 2], hidden[rows // 2 :]], axis=1)
-    out_ref[...] = jnp.broadcast_to(beside.astype(jnp.bfloat16)[None], out_ref.shape)
+    filled = jnp.concatenate([hidden, jnp.zeros((rows, alone - half), jnp.float32)], axis=1)
+    out_ref[...] = jnp.broadcast_to(filled.astype(jnp.bfloat16)[None], out_ref.shape)
 
 
 def gate_units(sums, units, model_width, copies):
-    half = units // 2
+    half, _, alone = widths(units)
     return pl.pallas_call(
         functools.partial(gate_kernel, half=half, model_width=model_width),
-        out_shape=pltpu.VMEM((copies, sums.shape[0] // 2, 2 * half), jnp.bfloat16),
+        out_shape=pltpu.VMEM((copies, sums.shape[0], alone), jnp.bfloat16),
         in_specs=whole(1),
         out_specs=pl.BlockSpec(memory_space=pltpu.VMEM),
         compiler_params=pltpu.CompilerParams(vmem_limit_bytes=8 << 20),
@@ -281,12 +281,11 @@
 
 def narrow_kernel(hidden, mine, got, out_ref, *, both):
     r = member(lax.axis_index("kv"))
-    half = hidden.shape[1] // 2
+    alone = hidden.shape[1]
     copies, width = out_ref.shape[1:3]
-    weights = jnp.concatenate([ref[:, both : both + half] for ref in (mine, got)], axis=0)
-    ordered = jnp.concatenate([hidden[:, :half], hidden[:, half:]], axis=0)
+    weights = jnp.concatenate([ref[:, both : both + alone] for ref in (mine, got)], axis=0)
     made = lax.dot_general(
-        weights, ordered, (((1,), (1,)), ((), ())), preferred_element_type=jnp.float32
+        weights, hidden[...], (((1,), (1,)), ((), ())), preferred_element_type=jnp.float32
     ).astype(jnp.bfloat16)
     for j in range(copies):
         out_ref[r, j] = made[:width]
@@ -294,7 +293,7 @@
 
 
 def narrow(hidden, mine, got, units, tp):
-    width, seqs = (mine.shape[0], 2 * hidden.shape[0])
+    width, seqs = (mine.shape[0], hidden.shape[0])
     return pl.pallas_call(
         functools.partial(narrow_kernel, both=widths(units)[1]),
         out_shape=pltpu.VMEM((2, tp, width, seqs), jnp.bfloat16),
@@ -361,7 +360,7 @@
     wide, mid_t = widen(attn_sums, mine, got, new_state, units, count)
     sums = summed(exchanged(wide, "kv", line))
     hidden = exchanged(gate_units(sums, units, model_width, count), "kv", line)
-    down_parts = narrow(hidden.reshape(-1, units), mine, got, units, tp).reshape(2 * tp, width, seqs)
+    down_parts = narrow(hidden.reshape(seqs, -1), mine, got, units, tp).reshape(2 * tp, width, seqs)
     mixed = (
         mid_t.astype(jnp.float32) + summed(exchanged(down_parts, ("kv", "tp"), pair))
     ).astype(jnp.bfloat16)

time: 127 us -> 126 us (level)
  no operation moved by 1% of the time
where the time goes in v1:
time: 126 us
  blocking collectives  82 us (65%)
  waiting for transfers between devices  19.5 us (15%)
  starting transfers between devices  17.2 us (14%)
  Pallas kernels  4.3 us (3%)
  other arithmetic  1.44 us (1%)
    all_to_all x4, blocking collectives, exchanged(): lax.all_to_all(blocks, axis, 0, 0, axis_index_groups=groups, tiled=True)  82 us
    all_to_all x2, waiting for transfers between devices, exchanged(): lax.all_to_all(blocks, axis, 0, 0, axis_index_groups=groups, tiled=True)  15.1 us
    all_to_all x2, starting transfers between devices, exchanged(): lax.all_to_all(blocks, axis, 0, 0, axis_index_groups=groups, tiled=True)  13.9 us
    ppermute x1, waiting for transfers between devices, local(): got = lax.ppermute(sent, 'kv', [(i, i ^ STRIDE) for i in range(kv)])  4.43 us
    ppermute x1, starting transfers between devices, local(): got = lax.ppermute(sent, 'kv', [(i, i ^ STRIDE) for i in range(kv)])  3.26 us
  transfers between devices with their start and end apart: 3, of which 3 were waited for; matrix products, arithmetic and copies ran while one was open for 0% of the time, Pallas kernels for 0%

profile of v1, /device:TPU:1, one launch (start us, length us, event | category | flops | bytes accessed | tf_op | source)
XLA Modules:
  0.0 125.5 jit_solution(14381669994555968895)
XLA Ops:
  0.6 1.3 %project.1 = (bf16[128,1920]{1,0:T(8,128)(2,1)S(1)}, f32[1,256]{1,0:T(1,128)S(1)}, bf16[4,128]{1,0:T(4,128)(2,1)S(1)}, bf16[1,64]{1,0:T(2,128)(2,1)S(1)}) custom-call(bf16[64,128]{1,0:T(8,128)(2,1)} %bitcast.15, bf16[1,64]{1,0:T(2,128)(2,1)} %bitcast.19, bf16[64,256]{1,0:T(8,128)(2,1)} %refs_2_.1, bf16[64,256]{1,0:T(8,128)(2,1)} %refs_3_.1, ...), custom_call_target="tpu_custom_call" | custom-call | tf_op jit(solution)/shard_map/project/pallas_call | solution.py:83
  1.9 0.0 copy-start
  2.0 0.2 reshape.36
  2.1 33.8 %all_to_all.30 = bf16[64,2,1920]{2,1,0:T(2,128)(2,1)S(1)} all-to-all(bf16[64,2,1920]{2,1,0:T(2,128)(2,1)S(1)} %reshape.36), channel_id=1, replica_groups=mesh['kv'=64,'tp'=8] {'kv'}, dimensions={0} | all-to-all | bytes 983040 | tf_op jit(solution)/shard_map/all_to_all | solution.py:308
  36.0 0.4 convert_reduce_fusion.sums
  36.4 0.0 copy-done
  36.4 1.2 attend.1
  37.6 6.5 %all-to-all-start.1 = ((bf16[64,2,512]{2,1,0:T(2,128)(2,1)}), bf16[64,2,512]{2,1,0:T(2,128)(2,1)S(1)}, u32[]{:S(2)}, u32[]{:S(2)}) async-start(bf16[64,2,512]{2,1,0:T(2,128)(2,1)} %get-tuple-element.19), calls=%async_computation.1 | async-start | bytes 262144 | tf_op jit(solution)/shard_map/all_to_all | solution.py:308
  44.1 0.2 multiply_add_fusion._
  44.3 0.0 copy-start.1
  44.3 0.0 copy-start.5
  44.3 11.3 %all-to-all-done.1 = bf16[64,2,512]{2,1,0:T(2,128)(2,1)S(1)} async-done(((bf16[64,2,512]{2,1,0:T(2,128)(2,1)}), bf16[64,2,512]{2,1,0:T(2,128)(2,1)S(1)}, u32[]{:S(2)}, u32[]{:S(2)}) %all-to-all-start.1) | async-done | bytes 131104 | tf_op jit(solution)/shard_map/all_to_all | solution.py:308
  55.6 0.1 reshape.37.heads
  55.7 0.0 copy-done.5
  55.7 0.0 copy-start.4
  55.7 0.9 join.1
  56.6 0.0 copy-start.2
  56.6 0.0 copy-start.3
  56.6 0.0 copy-start.6
  56.6 7.4 %all-to-all-start.2 = ((bf16[16,64,128]{2,1,0:T(8,128)(2,1)}), bf16[16,64,128]{2,1,0:T(8,128)(2,1)S(1)}, u32[]{:S(2)}, u32[]{:S(2)}) async-start(bf16[16,64,128]{2,1,0:T(8,128)(2,1)} %join.1), calls=%async_computation.2 | async-start | bytes 524288 | tf_op jit(solution)/shard_map/all_to_all | solution.py:308
  64.0 0.0 copy-done.4
  64.0 0.0 copy-done.2
  64.0 0.0 copy-done.3
  64.0 0.0 copy-done.6
  64.0 0.2 pack.1
  64.2 3.3 %collective-permute-start = (bf16[64,2432]{1,0:T(8,128)(2,1)S(1)}, bf16[64,2432]{1,0:T(8,128)(2,1)S(1)}, u32[]{:S(2)}, u32[]{:S(2)}) collective-permute-start(bf16[64,2432]{1,0:T(8,128)(2,1)S(1)} %get-tuple-element.26), channel_id=1, source_target_pairs={{0,64},{8,72},{16,80},{24,88},{32,96},{40,104},{48,112},{56,120},{... | collective-permute-start | bytes 933896 | tf_op jit(solution)/shard_map/ppermute | solution.py:347
  67.5 3.8 %all-to-all-done.2 = bf16[16,64,128]{2,1,0:T(8,128)(2,1)S(1)} async-done(((bf16[16,64,128]{2,1,0:T(8,128)(2,1)}), bf16[16,64,128]{2,1,0:T(8,128)(2,1)S(1)}, u32[]{:S(2)}, u32[]{:S(2)}) %all-to-all-start.2) | async-done | bytes 262176 | tf_op jit(solution)/shard_map/all_to_all | solution.py:308
  71.3 4.4 %collective-permute-done.got = bf16[64,2432]{1,0:T(8,128)(2,1)S(1)} collective-permute-done((bf16[64,2432]{1,0:T(8,128)(2,1)S(1)}, bf16[64,2432]{1,0:T(8,128)(2,1)S(1)}, u32[]{:S(2)}, u32[]{:S(2)}) %collective-permute-start) | collective-permute-done | bytes 311328 | tf_op jit(solution)/shard_map/ppermute | solution.py:347
  75.7 0.0 copy-done.1
  75.7 0.3 widen.1
  76.1 15.7 %all_to_all.31 = bf16[32,4,1408]{2,1,0:T(4,128)(2,1)S(1)} all-to-all(bf16[32,4,1408]{2,1,0:T(4,128)(2,1)S(1)} %get-tuple-element.29), channel_id=1, replica_groups={{0,8,16,24,32,40,48,56,128,136,144,152,160,168,176,184,320,328,336,344,..., dimensions={0} | all-to-all | bytes 720896 | tf_op jit(solution)/shard_map/all_to_all | solution.py:308
  91.8 0.2 convert_reduce_fusion.1.sums
  92.0 0.2 gate.1
  92.1 18.2 %all_to_all.32 = bf16[32,4,768]{2,1,0:T(4,128)(2,1)S(1)} all-to-all(bf16[32,4,768]{2,1,0:T(4,128)(2,1)S(1)} %gate.1), channel_id=1, replica_groups={{0,8,16,24,32,40,48,56,128,136,144,152,160,168,176,184,320,328,336,344,..., dimensions={0} | all-to-all | bytes 393216 | tf_op jit(solution)/shard_map/all_to_all | solution.py:308
  110.3 0.1 reshape.39.hidden
  110.4 0.2 narrow.1
  110.6 14.3 %all_to_all.33 = bf16[16,64,128]{2,1,0:T(8,128)(2,1)S(1)} all-to-all(bf16[16,64,128]{2,1,0:T(8,128)(2,1)S(1)} %bitcast.12), channel_id=1, replica_groups={{0,1,2,3,4,5,6,7,64,65,66,67,68,69,70,71},{8,9,10,11,12,13,14,15,72,73,..., dimensions={0} | all-to-all | bytes 524288 | tf_op jit(solution)/shard_map/all_to_all | solution.py:308
  124.9 0.6 fusion
  (2 shorter events, 0.1 us)
Async XLA Ops:
  1.9 34.4 %copy-start = (f32[2,1,256,512]{3,2,1,0:T(8,128)S(1)}, f32[2,1,256,512]{3,2,1,0:T(8,128)}, u32[]{:S(2)}) copy-start(f32[2,1,256,512]{3,2,1,0:T(8,128)} %state.1) | copy-start | bytes 3145732
  37.6 18.0 %all-to-all-start.1 = ((bf16[64,2,512]{2,1,0:T(2,128)(2,1)}), bf16[64,2,512]{2,1,0:T(2,128)(2,1)S(1)}, u32[]{:S(2)}, u32[]{:S(2)}) async-start(bf16[64,2,512]{2,1,0:T(2,128)(2,1)} %get-tuple-element.19), calls=%async_computation.1 | async-start | bytes 262144 | tf_op jit(solution)/shard_map/all_to_all | solution.py:308
  44.3 31.4 %copy-start.1 = (f32[2,1,256,512]{3,2,1,0:T(8,128)}, f32[2,1,256,512]{3,2,1,0:T(8,128)S(1)}, u32[]{:S(2)}) copy-start(f32[2,1,256,512]{3,2,1,0:T(8,128)S(1)} %multiply_add_fusion._) | copy-start | bytes 3145732
  44.3 11.4 %copy-start.5 = (bf16[512,64]{0,1:T(8,128)(2,1)S(1)}, bf16[512,64]{0,1:T(8,128)(2,1)}, u32[]{:S(2)}) copy-start(bf16[512,64]{0,1:T(8,128)(2,1)} %param.25) | copy-start | bytes 196612
  55.7 8.3 %copy-start.4 = (bf16[1376,64]{0,1:T(8,128)(2,1)S(1)}, bf16[1376,64]{0,1:T(8,128)(2,1)}, u32[]{:S(2)}) copy-start(bf16[1376,64]{0,1:T(8,128)(2,1)} %param.28) | copy-start | bytes 528388
  56.6 7.4 %copy-start.2 = (bf16[64,1376]{1,0:T(8,128)(2,1)S(1)}, bf16[64,1376]{1,0:T(8,128)(2,1)}, u32[]{:S(2)}) copy-start(bf16[64,1376]{1,0:T(8,128)(2,1)} %refs_0_.1) | copy-start | bytes 528388
  56.6 7.5 %copy-start.3 = (bf16[64,1376]{1,0:T(8,128)(2,1)S(1)}, bf16[64,1376]{1,0:T(8,128)(2,1)}, u32[]{:S(2)}) copy-start(bf16[64,1376]{1,0:T(8,128)(2,1)} %refs_1_.1) | copy-start | bytes 528388
  56.6 7.5 %copy-start.6 = (bf16[128,64]{0,1:T(8,128)(2,1)S(1)}, bf16[128,64]{0,1:T(8,128)(2,1)}, u32[]{:S(2)}) copy-start(bf16[128,64]{0,1:T(8,128)(2,1)} %param.15) | copy-start | bytes 49156
  56.6 14.7 %all-to-all-start.2 = ((bf16[16,64,128]{2,1,0:T(8,128)(2,1)}), bf16[16,64,128]{2,1,0:T(8,128)(2,1)S(1)}, u32[]{:S(2)}, u32[]{:S(2)}) async-start(bf16[16,64,128]{2,1,0:T(8,128)(2,1)} %join.1), calls=%async_computation.2 | async-start | bytes 524288 | tf_op jit(solution)/shard_map/all_to_all | solution.py:308
  64.2 11.5 %collective-permute-start = (bf16[64,2432]{1,0:T(8,128)(2,1)S(1)}, bf16[64,2432]{1,0:T(8,128)(2,1)S(1)}, u32[]{:S(2)}, u32[]{:S(2)}) collective-permute-start(bf16[64,2432]{1,0:T(8,128)(2,1)S(1)} %get-tuple-element.26), channel_id=1, source_target_pairs={{0,64},{8,72},{16,80},{24,88},{32,96},{40,104},{48,112},{56,120},{... | collective-permute-start | bytes 933896 | tf_op jit(solution)/shard_map/ppermute | solution.py:347
